TPU v7x, 32 devices: a whole 2x2x4 slice. The times are simulated.
32 devices in a mesh: ep: 8 (over z, y), tp: 4 (over x, core).
Axes of the slice: x: 2, y: 2, z: 4, core: 2. Of those that a mesh axis runs over, the one named last changes fastest.
Arguments:
- queries: bfloat16 [4096, 1024], P('ep', 'tp'), may hold values from -10.5 to 10.5
- keys: bfloat16 [4096, 512], P('ep', 'tp'), may hold values from -10.5 to 10.5
- values: bfloat16 [4096, 512], P('ep', 'tp'), may hold values from -6 to 6
- head_lambda: float32 [8], P('tp'), may hold values from 0.3 to 0.8
- out_gain: float32 [128], replicated, may hold values from 0.1 to 1.9
- expert_input: bfloat16 [4096, 2048], P(('ep', 'tp')), may hold values from -6 to 6
- routes: int32 [4096, 4], P(('ep', 'tp')), may hold values from 0 to 7, all different within a row; in each aligned block of 128 rows (0 to 127, 128 to 255, ...) at most 80 rows name the same one
- route_weight: float32 [4096, 4], P(('ep', 'tp')), may hold values from 0.2 to 0.6
- moe_gain: float32 [2048], replicated, may hold values from 0.1 to 1.9
- gate_weight: bfloat16 [8, 2048, 2048], P('ep', None, 'tp'), may hold values from -0.3125 to 0.3125
- up_weight: bfloat16 [8, 2048, 2048], P('ep', None, 'tp'), may hold values from -0.3125 to 0.3125
- down_weight: bfloat16 [8, 2048, 2048], P('ep', 'tp'), may hold values from -0.03125 to 0.03125
Outputs:
- mixed_out: bfloat16 [4096, 1024], P('ep', 'tp')
- expert_mix: bfloat16 [4096, 2048], P(('ep', 'tp'))
Inputs may be any that keep to these rules, and one draw needn't show every extreme that they name: `routes`: each row names 4 different experts. Among the rows of one device (aligned blocks of 128 rows) no expert is named more than 80 times, and in some blocks one is named exactly 80 times.
All inputs are finite; a program needn't handle non-finite values.
Results may differ from a plain program's by a relative error of at most 0.012.
Values may be sent and summed in bfloat16 or wider, within the bound.
A program may use at most 128 MiB of HBM per device.

v0:
```python
import math

import jax
import jax.numpy as jnp
from jax import lax
from jax.sharding import PartitionSpec as P

HEADS = 8
KV_HEADS = 4
HEAD = 64
VDIM = 128


epsilon = 1e-05


def expert_act(rows_in, gate_matrix, up_matrix):
    gate_pre = jnp.dot(rows_in, gate_matrix, preferred_element_type=jnp.float32)
    up_pre = jnp.dot(rows_in, up_matrix, preferred_element_type=jnp.float32)
    clipped = jnp.minimum(gate_pre, 7.0)
    up_clip = jnp.clip(up_pre, -7.0, 7.0)
    return ((up_clip + 1.0) * clipped * jax.nn.sigmoid(1.702 * clipped)).astype(jnp.bfloat16)


def shards(
    queries,
    keys,
    values,
    head_lambda,
    out_gain,
    expert_input,
    routes,
    route_weight,
    moe_gain,
    gate_weight,
    up_weight,
    down_weight,
):
    seq_rows = queries.shape[0]
    kv_local = keys.shape[1] // (2 * HEAD)
    group_size = HEADS // KV_HEADS
    query_start = lax.axis_index("ep") * seq_rows
    score_scale = HEAD ** (-0.5)
    query_sets = [(queries, query_start + jnp.arange(seq_rows, dtype=jnp.int32))]
    set_views = [
        rows.reshape(rows.shape[0], kv_local, group_size, 2, HEAD) for rows, unused in query_sets
    ]
    set_positions = [positions for unused, positions in query_sets]
    set_last = [positions[-1] for positions in set_positions]

    def update(running, query_view, query_pos, key_block, value_block, key_start):
        run_max, run_total, run_sum = running
        scores = (
            jnp.einsum(
                "tkgmd,skmd->mtkgs", query_view, key_block, preferred_element_type=jnp.float32
            )
            * score_scale
        )
        key_pos = key_start + jnp.arange(key_block.shape[0], dtype=jnp.int32)
        allowed = (key_pos[None, :] <= query_pos[:, None])[None, :, None, None, :]
        block_max = jnp.max(jnp.where(allowed, scores, -jnp.inf), axis=-1)
        new_max = jnp.maximum(run_max, block_max)
        weights = jnp.where(allowed, jnp.exp(scores - new_max[..., None]), 0.0)
        factor = jnp.exp(run_max - new_max)
        new_total = factor * run_total + jnp.sum(weights, axis=-1)
        new_sum = factor[..., None] * run_sum + jnp.einsum(
            "ournf,frj->ournj",
            weights.astype(jnp.bfloat16),
            value_block,
            preferred_element_type=jnp.float32,
        )
        return (new_max, new_total, new_sum)

    initial = tuple(
        (
            (
                jnp.full((2, view.shape[0], kv_local, group_size), -1e30, jnp.float32),
                jnp.zeros((2, view.shape[0], kv_local, group_size), jnp.float32),
                jnp.zeros((2, view.shape[0], kv_local, group_size, VDIM), jnp.float32),
            )
            for view in set_views
        )
    )
    key_piece = lax.all_gather(keys, "ep", axis=0, tiled=True)
    value_piece = lax.all_gather(values, "ep", axis=0, tiled=True)
    piece_rows = key_piece.shape[0]
    block_len = math.gcd(piece_rows, 512)
    key_view = key_piece.reshape(piece_rows, kv_local, 2, HEAD)
    value_view = value_piece.reshape(piece_rows, kv_local, VDIM)

    def block_step(block_index, inner_state):
        offset = block_index * block_len
        key_block = lax.dynamic_slice_in_dim(key_view, offset, block_len, 0)
        value_block = lax.dynamic_slice_in_dim(value_view, offset, block_len, 0)
        set_index = 0

        def compute(current, set_index=set_index):
            return update(
                current,
                set_views[set_index],
                set_positions[set_index],
                key_block,
                value_block,
                offset,
            )

        results = [
            lax.cond(
                offset <= set_last[set_index],
                compute,
                lambda unchanged: unchanged,
                inner_state[set_index],
            )
        ]
        return tuple(results)

    folded = lax.fori_loop(0, piece_rows // block_len, block_step, initial)
    lambdas = head_lambda.reshape(kv_local, group_size)[None, :, :, None]
    finished = []
    for run_max, run_total, run_sum in folded:
        combined = (
            run_sum[0] / run_total[0][..., None] - lambdas * run_sum[1] / run_total[1][..., None]
        )
        inverse_rms = lax.rsqrt(jnp.mean(combined * combined, axis=-1, keepdims=True) + epsilon)
        finished.append(
            (combined * inverse_rms * out_gain)
            .astype(jnp.bfloat16)
            .reshape(combined.shape[0], kv_local * group_size * VDIM)
        )
    mixed_out = finished[0]
    token_count = expert_input.shape[0]
    top_count = routes.shape[1]
    model_width = expert_input.shape[1]
    ep_count = lax.axis_size("ep")
    capacity = 5 * token_count * top_count // (4 * ep_count)
    inputs_f32 = expert_input.astype(jnp.float32)
    normed = (
        inputs_f32
        * lax.rsqrt(jnp.mean(inputs_f32 * inputs_f32, axis=-1, keepdims=True) + epsilon)
        * moe_gain
    ).astype(jnp.bfloat16)
    flat_routes = routes.reshape(-1)
    route_total = flat_routes.shape[0]
    one_hot = (flat_routes[:, None] == jnp.arange(ep_count, dtype=jnp.int32)[None, :]).astype(
        jnp.int32
    )
    slot_rank = jnp.sum(jnp.cumsum(one_hot, axis=0) * one_hot, axis=1) - 1
    target = flat_routes * capacity + slot_rank
    slot_token = (
        jnp.zeros((ep_count * capacity,), jnp.int32)
        .at[target]
        .set(jnp.arange(route_total, dtype=jnp.int32) // top_count)
    )
    slot_live = jnp.zeros((ep_count * capacity,), jnp.bool_).at[target].set(True)
    outgoing = jnp.where(slot_live[:, None], normed[slot_token], jnp.zeros((), jnp.bfloat16))
    local_gate = gate_weight[0]
    local_up = up_weight[0]
    local_down = down_weight[0]
    arrived = lax.all_to_all(outgoing, "ep", split_axis=0, concat_axis=0, tiled=True)
    activated = expert_act(lax.all_gather(arrived, "tp", axis=0, tiled=True), local_gate, local_up)
    summed = lax.psum_scatter(
        jnp.dot(activated, local_down, preferred_element_type=jnp.float32).astype(jnp.bfloat16),
        "tp",
        scatter_dimension=0,
        tiled=True,
    )
    returned = lax.all_to_all(summed, "ep", split_axis=0, concat_axis=0, tiled=True)
    picked = returned[target].reshape(token_count, top_count, model_width).astype(jnp.float32)
    expert_mix = jnp.sum(route_weight[:, :, None] * picked, axis=1).astype(jnp.bfloat16)
    return (mixed_out, expert_mix)


def solution(mesh):
    placed = (
        P("ep", "tp"),
        P("ep", "tp"),
        P("ep", "tp"),
        P("tp"),
        P(),
        P(("ep", "tp"), None),
        P(("ep", "tp"), None),
        P(("ep", "tp"), None),
        P(),
        P("ep", None, "tp"),
        P("ep", None, "tp"),
        P("ep", "tp", None),
    )
    return jax.shard_map(
        shards,
        mesh=mesh,
        in_specs=placed,
        out_specs=(P("ep", "tp"), P(("ep", "tp"), None)),
        check_vma=False,
    )
```

profile of v0, /device:TPU:28, one launch (start us, length us, event | category | flops | bytes accessed | tf_op | source)
XLA Modules:
  0.0 419.5 jit_solution(7746177447401328933)
XLA Ops:
  11.6 2.4 scatter_custom_fusion.1
  15.4 2.4 scatter_custom_fusion
  19.2 4.1 gather_fusion
  25.2 63.0 %all_to_all.21 = bf16[8,80,2048]{2,1,0:T(8,128)(2,1)} all-to-all(bf16[8,80,2048]{2,1,0:T(8,128)(2,1)S(1)} %broadcast_select_fusion), channel_id=1, replica_groups=mesh['ep'=8,'tp'=4] {'ep'}, dimensions={0} | all-to-all | bytes 5242880 | tf_op jit(solution)/shard_map/all_to_all | solution.py:159
  88.5 71.0 %all-gather.8.cloned.1.call-done = bf16[2560,2048]{1,0:T(8,128)(2,1)} async-done(((bf16[640,2048]{1,0:T(8,128)(2,1)}), bf16[2560,2048]{1,0:T(8,128)(2,1)}) %all-gather.8.cloned.1.call-update) | async-done | bytes 10485776 | tf_op jit(solution)/shard_map/all_gather | solution.py:160
  159.5 10.5 %convolution_clamp_fusion = f32[2560,512]{1,0:T(8,128)} fusion(bf16[2560,2048]{1,0:T(8,128)(2,1)} %all-gather.8.cloned.1.call-done, bf16[1,2048,512]{2,1,0:T(8,128)(2,1)} %param.26), kind=kOutput, calls=%fused_computation.35 | convolution fusion | flops 5370019840 | bytes 17825792 | tf_op jit(solution)/shard_map/dot_general | solution.py:19
  170.0 18.4 %convolution_convert_fusion = bf16[2560,2048]{1,0:T(8,128)(2,1)} fusion(f32[2560,512]{1,0:T(8,128)} %convolution_clamp_fusion, bf16[2560,2048]{1,0:T(8,128)(2,1)} %all-gather.8.cloned.1.call-done, bf16[1,512,2048]{2,1,0:T(8,128)(2,1)S(1)} %copy-done, bf16[1,2048,512]{2,1,0:T(8,128)(2,1)} %param.25), kind=kOutput, calls=%fused_computation.34 | convolution fusion | flops 10754457600 | bytes 30408704 | tf_op jit(solution)/shard_map/dot_general | solution.py:162
  189.1 83.9 %reduce-scatter.2.cloned.1.call-done = bf16[640,2048]{1,0:T(8,128)(2,1)} async-done(((bf16[2560,2048]{1,0:T(8,128)(2,1)}), bf16[640,2048]{1,0:T(8,128)(2,1)}) %reduce-scatter.2.cloned.1.call-update) | async-done | bytes 2621456 | tf_op jit(solution)/shard_map/reduce_scatter | solution.py:161
  273.0 6.0 %all-to-all-start.1 = ((bf16[8,80,2048]{2,1,0:T(8,128)(2,1)}), bf16[8,80,2048]{2,1,0:T(8,128)(2,1)}, u32[]{:S(2)}, u32[]{:S(2)}) async-start(bf16[8,80,2048]{2,1,0:T(8,128)(2,1)} %bitcast.143), calls=%async_computation.2 | async-start | bytes 5242880 | tf_op jit(solution)/shard_map/all_to_all | solution.py:167
  282.5 66.2 %all-gather.6.cloned.1.call-done = bf16[4096,128]{0,1:T(8,128)(2,1)} async-done(((bf16[512,128]{0,1:T(8,128)(2,1)}), bf16[4096,128]{0,1:T(8,128)(2,1)}) %all-gather.6.cloned.1.call-update) | async-done | bytes 1048592 | tf_op jit(solution)/shard_map/all_gather | solution.py:85
  348.8 40.9 %while.18 = (s32[]{:T(128)}, f32[2,512,1,2]{1,3,0,2:T(2,128)S(1)}, f32[2,512,1,2]{1,3,0,2:T(2,128)S(1)}, f32[2,512,1,2,128]{1,4,3,0,2:T(8,128)S(1)}, s32[]{:T(12...) while((s32[]{:T(128)}, f32[2,512,1,2]{1,3,0,2:T(2,128)S(1)}, ...), condition=%wide.region_5.6_spmd.clone, body=%wide.region_0.5_spmd.clone.sunk | while | flops 414981120 | bytes 16396601 | solution.py:117
  349.6 4.4 %conditional.3 = ((f32[2,512,1,2]{1,3,0,2:T(2,128)S(1)}, f32[2,512,1,2]{1,3,0,2:T(2,128)S(1)}, f32[2,512,1,2,128]{1,4,3,0,2:T(8,128)S(1)})) conditional(s32[]{:T(128)} %convert_element_type.80, (f32[2,512,1,2]{1,3,0,2:T(2,128)S(1)}, f32[2,512,1,2]{1,3,0,2:T(2,128)S(1)}, f32[2,512,1,2,128]{1,4,3,0,2:T(8,128)S(1)}) %tuple.62, (s32[]{:T(128)}, ...), branch_computations={%region_1.0_spmd, %region_2.4_spmd} | conditional | flops 414981120 | bytes 16394322 | solution.py:108
  354.7 4.4 %conditional.3 = ((f32[2,512,1,2]{1,3,0,2:T(2,128)S(1)}, f32[2,512,1,2]{1,3,0,2:T(2,128)S(1)}, f32[2,512,1,2,128]{1,4,3,0,2:T(8,128)S(1)})) conditional(s32[]{:T(128)} %convert_element_type.80, (f32[2,512,1,2]{1,3,0,2:T(2,128)S(1)}, f32[2,512,1,2]{1,3,0,2:T(2,128)S(1)}, f32[2,512,1,2,128]{1,4,3,0,2:T(8,128)S(1)}) %tuple.62, (s32[]{:T(128)}, ...), branch_computations={%region_1.0_spmd, %region_2.4_spmd} | conditional | flops 414981120 | bytes 16394322 | solution.py:108
  359.8 4.4 %conditional.3 = ((f32[2,512,1,2]{1,3,0,2:T(2,128)S(1)}, f32[2,512,1,2]{1,3,0,2:T(2,128)S(1)}, f32[2,512,1,2,128]{1,4,3,0,2:T(8,128)S(1)})) conditional(s32[]{:T(128)} %convert_element_type.80, (f32[2,512,1,2]{1,3,0,2:T(2,128)S(1)}, f32[2,512,1,2]{1,3,0,2:T(2,128)S(1)}, f32[2,512,1,2,128]{1,4,3,0,2:T(8,128)S(1)}) %tuple.62, (s32[]{:T(128)}, ...), branch_computations={%region_1.0_spmd, %region_2.4_spmd} | conditional | flops 414981120 | bytes 16394322 | solution.py:108
  364.9 4.4 %conditional.3 = ((f32[2,512,1,2]{1,3,0,2:T(2,128)S(1)}, f32[2,512,1,2]{1,3,0,2:T(2,128)S(1)}, f32[2,512,1,2,128]{1,4,3,0,2:T(8,128)S(1)})) conditional(s32[]{:T(128)} %convert_element_type.80, (f32[2,512,1,2]{1,3,0,2:T(2,128)S(1)}, f32[2,512,1,2]{1,3,0,2:T(2,128)S(1)}, f32[2,512,1,2,128]{1,4,3,0,2:T(8,128)S(1)}) %tuple.62, (s32[]{:T(128)}, ...), branch_computations={%region_1.0_spmd, %region_2.4_spmd} | conditional | flops 414981120 | bytes 16394322 | solution.py:108
  366.1 2.3 fusion.14
  370.0 4.4 %conditional.3 = ((f32[2,512,1,2]{1,3,0,2:T(2,128)S(1)}, f32[2,512,1,2]{1,3,0,2:T(2,128)S(1)}, f32[2,512,1,2,128]{1,4,3,0,2:T(8,128)S(1)})) conditional(s32[]{:T(128)} %convert_element_type.80, (f32[2,512,1,2]{1,3,0,2:T(2,128)S(1)}, f32[2,512,1,2]{1,3,0,2:T(2,128)S(1)}, f32[2,512,1,2,128]{1,4,3,0,2:T(8,128)S(1)}) %tuple.62, (s32[]{:T(128)}, ...), branch_computations={%region_1.0_spmd, %region_2.4_spmd} | conditional | flops 414981120 | bytes 16394322 | solution.py:108
  375.1 4.4 %conditional.3 = ((f32[2,512,1,2]{1,3,0,2:T(2,128)S(1)}, f32[2,512,1,2]{1,3,0,2:T(2,128)S(1)}, f32[2,512,1,2,128]{1,4,3,0,2:T(8,128)S(1)})) conditional(s32[]{:T(128)} %convert_element_type.80, (f32[2,512,1,2]{1,3,0,2:T(2,128)S(1)}, f32[2,512,1,2]{1,3,0,2:T(2,128)S(1)}, f32[2,512,1,2,128]{1,4,3,0,2:T(8,128)S(1)}) %tuple.62, (s32[]{:T(128)}, ...), branch_computations={%region_1.0_spmd, %region_2.4_spmd} | conditional | flops 414981120 | bytes 16394322 | solution.py:108
  380.2 4.4 %conditional.3 = ((f32[2,512,1,2]{1,3,0,2:T(2,128)S(1)}, f32[2,512,1,2]{1,3,0,2:T(2,128)S(1)}, f32[2,512,1,2,128]{1,4,3,0,2:T(8,128)S(1)})) conditional(s32[]{:T(128)} %convert_element_type.80, (f32[2,512,1,2]{1,3,0,2:T(2,128)S(1)}, f32[2,512,1,2]{1,3,0,2:T(2,128)S(1)}, f32[2,512,1,2,128]{1,4,3,0,2:T(8,128)S(1)}) %tuple.62, (s32[]{:T(128)}, ...), branch_computations={%region_1.0_spmd, %region_2.4_spmd} | conditional | flops 414981120 | bytes 16394322 | solution.py:108
  385.3 4.4 %conditional.3 = ((f32[2,512,1,2]{1,3,0,2:T(2,128)S(1)}, f32[2,512,1,2]{1,3,0,2:T(2,128)S(1)}, f32[2,512,1,2,128]{1,4,3,0,2:T(8,128)S(1)})) conditional(s32[]{:T(128)} %convert_element_type.80, (f32[2,512,1,2]{1,3,0,2:T(2,128)S(1)}, f32[2,512,1,2]{1,3,0,2:T(2,128)S(1)}, f32[2,512,1,2,128]{1,4,3,0,2:T(8,128)S(1)}) %tuple.62, (s32[]{:T(128)}, ...), branch_computations={%region_1.0_spmd, %region_2.4_spmd} | conditional | flops 414981120 | bytes 16394322 | solution.py:108
  386.5 2.3 fusion.14
  393.6 7.5 %gather_fusion.1 = bf16[512,2048]{1,0:T(8,128)(2,1)} fusion(bf16[640,2048]{1,0:T(8,128)(2,1)} %bitcast.40, s32[1024]{0:T(1024)S(1)} %pad_clamp_fusion), kind=kCustom, calls=%fused_computation.1 | custom fusion | bytes 4196352 | tf_op jit(solution)/shard_map/gather | solution.py:168
  401.1 4.8 %reshape.254 = f32[128,4,2048]{2,1,0:T(4,128)} reshape(bf16[512,2048]{1,0:T(8,128)(2,1)} %gather_fusion.1) | data formatting | bytes 6291456 | tf_op jit(solution)/shard_map/convert_element_type | solution.py:168
  405.9 6.2 %multiply_reduce_fusion = bf16[128,2048]{1,0:T(8,128)(2,1)} fusion(f32[128,4,2048]{2,1,0:T(4,128)} %reshape.254, f32[128,4]{1,0:T(8,128)S(1)} %copy.48), kind=kLoop, calls=%fused_computation.37 | loop fusion | flops 1835008 | bytes 4720640 | tf_op jit(solution)/shard_map/reduce_sum | solution.py:169
  (143 shorter events, 46.5 us)
Async XLA Ops:
  8.0 162.0 %copy-start = (bf16[1,512,2048]{2,1,0:T(8,128)(2,1)S(1)}, bf16[1,512,2048]{2,1,0:T(8,128)(2,1)}, u32[]{:S(2)}) copy-start(bf16[1,512,2048]{2,1,0:T(8,128)(2,1)} %param.27) | copy-start | bytes 6291460
  8.0 151.5 %all-gather.8.cloned.1.call-start = ((), (), s32[]{:S(2)}) async-start(), calls=%async_computation.5 | async-start | bytes 13107200 | tf_op jit(solution)/shard_map/all_gather | solution.py:160
  88.2 184.7 %reduce-scatter.2.cloned.1.call-start = ((), (), s32[]{:S(2)}) async-start(), calls=%async_computation.6 | async-start | bytes 13107200 | tf_op jit(solution)/shard_map/reduce_scatter | solution.py:161
  188.4 90.6 %copy-start.3 = (bf16[512,128]{1,0:T(8,128)(2,1)S(1)}, bf16[512,128]{1,0:T(8,128)(2,1)}, u32[]{:S(2)}) copy-start(bf16[512,128]{1,0:T(8,128)(2,1)} %param.18) | copy-start | bytes 393220
  188.4 92.0 %copy-start.2 = (bf16[512,256]{1,0:T(8,128)(2,1)S(1)}, bf16[512,256]{1,0:T(8,128)(2,1)}, u32[]{:S(2)}) copy-start(bf16[512,256]{1,0:T(8,128)(2,1)} %param.16) | copy-start | bytes 786436
  188.4 92.2 %copy-start.5 = (f32[128,4]{0,1:T(4,128)S(1)}, f32[128,4]{0,1:T(4,128)}, u32[]{:S(2)}) copy-start(f32[128,4]{0,1:T(4,128)} %param.23) | copy-start | bytes 6148
  188.4 92.3 %copy-start.4 = (f32[2]{0:T(128)S(1)}, f32[2]{0:T(128)}, u32[]{:S(2)}) copy-start(f32[2]{0:T(128)} %param.19) | copy-start | bytes 28
  188.5 92.3 %copy-start.6 = (f32[128]{0:T(128)S(1)}, f32[128]{0:T(128)}, u32[]{:S(2)}) copy-start(f32[128]{0:T(128)} %param.20) | copy-start | bytes 1540
  188.5 92.4 %all-gather.4.cloned.1.call-start = ((), (), s32[]{:S(2)}) async-start(), calls=%async_computation.3 | async-start | bytes 1179648 | tf_op jit(solution)/shard_map/all_gather | solution.py:84
  273.0 120.6 %all-to-all-start.1 = ((bf16[8,80,2048]{2,1,0:T(8,128)(2,1)}), bf16[8,80,2048]{2,1,0:T(8,128)(2,1)}, u32[]{:S(2)}, u32[]{:S(2)}) async-start(bf16[8,80,2048]{2,1,0:T(8,128)(2,1)} %bitcast.143), calls=%async_computation.2 | async-start | bytes 5242880 | tf_op jit(solution)/shard_map/all_to_all | solution.py:167
  279.0 69.7 %all-gather.6.cloned.1.call-start = ((), (), s32[]{:S(2)}) async-start(), calls=%async_computation.4 | async-start | bytes 1179648 | tf_op jit(solution)/shard_map/all_gather | solution.py:85
  393.6 18.5 %copy-start.1 = (bf16[1,512,2048]{2,1,0:T(8,128)(2,1)S(1)}, bf16[1,512,2048]{2,1,0:T(8,128)(2,1)}, u32[]{:S(2)}) copy-start(bf16[1,512,2048]{2,1,0:T(8,128)(2,1)} %param.27) | copy-start | bytes 6291460
Sparse Core Ops, SparseCore 0:
  88.3 71.0 all-gather.7
  188.5 84.3 reduce-scatter.1
Sparse Core Ops, SparseCore 1:
  191.1 38.0 all-gather.3
  282.1 66.6 all-gather.5
where the time goes:
time: 420 us; the launch traced here: 419 us
  waiting for transfers between devices  222 us (53%)
  blocking collectives  63 us (15%)
  matrix products  54 us (13%)
  local copies, waits for them, and re-layouts  29.3 us (7%)
  other arithmetic  23.2 us (6%)
  between operations  15.8 us (4%)
  loops' own time  6.32 us (2%)
  starting transfers between devices  6.3 us (2%)
    reduce_scatter x1, waiting for transfers between devices, shards(): lax.psum_scatter(jnp.dot(activated, local_down, preferred_element_type=jn...  83.9 us
    all_gather x1, waiting for transfers between devices, shards(): lax.all_gather(arrived, 'tp', axis=0, tiled=True)  71 us
    all_gather x1, waiting for transfers between devices, shards(): value_piece = lax.all_gather(values, 'ep', axis=0, tiled=True)  66.2 us
    all_to_all x1, blocking collectives, shards(): lax.all_to_all(outgoing, 'ep', split_axis=0, concat_axis=0, tiled=True)  63 us
    dot_general x1, matrix products, shards(): jnp.dot(activated, local_down, preferred_element_type=jnp.float32)  18.4 us
    dot_general x8, matrix products, update(): jnp.einsum('ournf,frj->ournj', weights.astype(jnp.bfloat16), value_block,...  18 us
    dot_general x1, matrix products, expert_act(): up_pre = jnp.dot(rows_in, up_matrix, preferred_element_type=jnp.float32)  10.5 us
  transfers between devices with their start and end apart: 5, of which 3 were waited for; matrix products, arithmetic and copies ran while one was open for 10% of the time, Pallas kernels for 0%

commit v1 on v0

v1 whole, which is shorter than its diff:
```python
import functools
import math

import jax
import jax.numpy as jnp
from jax import lax
from jax.experimental import pallas as pl
from jax.experimental.pallas import tpu as pltpu
from jax.sharding import PartitionSpec as P

HEADS = 8
KV_HEADS = 4
HEAD = 64
VDIM = 128


epsilon = 1e-05


def expert_act(rows_in, gate_matrix, up_matrix):
    gate_pre = jnp.dot(rows_in, gate_matrix, preferred_element_type=jnp.float32)
    up_pre = jnp.dot(rows_in, up_matrix, preferred_element_type=jnp.float32)
    clipped = jnp.minimum(gate_pre, 7.0)
    up_clip = jnp.clip(up_pre, -7.0, 7.0)
    return ((up_clip + 1.0) * clipped * jax.nn.sigmoid(1.702 * clipped)).astype(jnp.bfloat16)


def routed_experts(
    expert_input, routes, route_weight, moe_gain, gate_weight, up_weight, down_weight
):
    token_count = expert_input.shape[0]
    top_count = routes.shape[1]
    model_width = expert_input.shape[1]
    ep_count = lax.axis_size("ep")
    capacity = 5 * token_count * top_count // (4 * ep_count)
    inputs_f32 = expert_input.astype(jnp.float32)
    normed = (
        inputs_f32
        * lax.rsqrt(jnp.mean(inputs_f32 * inputs_f32, axis=-1, keepdims=True) + epsilon)
        * moe_gain
    ).astype(jnp.bfloat16)
    flat_routes = routes.reshape(-1)
    route_total = flat_routes.shape[0]
    one_hot = (flat_routes[:, None] == jnp.arange(ep_count, dtype=jnp.int32)[None, :]).astype(
        jnp.int32
    )
    slot_rank = jnp.sum(jnp.cumsum(one_hot, axis=0) * one_hot, axis=1) - 1
    target = flat_routes * capacity + slot_rank
    slot_token = (
        jnp.zeros((ep_count * capacity,), jnp.int32)
        .at[target]
        .set(jnp.arange(route_total, dtype=jnp.int32) // top_count)
    )
    slot_live = jnp.zeros((ep_count * capacity,), jnp.bool_).at[target].set(True)
    outgoing = jnp.where(slot_live[:, None], normed[slot_token], jnp.zeros((), jnp.bfloat16))
    local_gate = gate_weight[0]
    local_up = up_weight[0]
    local_down = down_weight[0]
    arrived = lax.all_to_all(outgoing, "ep", split_axis=0, concat_axis=0, tiled=True)
    activated = expert_act(lax.all_gather(arrived, "tp", axis=0, tiled=True), local_gate, local_up)
    summed = lax.psum_scatter(
        jnp.dot(activated, local_down, preferred_element_type=jnp.float32).astype(jnp.bfloat16),
        "tp",
        scatter_dimension=0,
        tiled=True,
    )
    returned = lax.all_to_all(summed, "ep", split_axis=0, concat_axis=0, tiled=True)
    picked = returned[target].reshape(token_count, top_count, model_width).astype(jnp.float32)
    expert_mix = jnp.sum(route_weight[:, :, None] * picked, axis=1).astype(jnp.bfloat16)
    return expert_mix


def attention_kernel(
    block_len, start_ref, lambda_ref, query_ref, kv_ref, gain_ref, out_ref, spread, sums, peaks
):
    rows = query_ref.shape[0]
    width = 2 * HEAD
    heads = query_ref.shape[1] // width
    kv_heads = kv_ref.shape[1] // (width + VDIM)
    group_size = heads // kv_heads
    lane = lax.broadcasted_iota(jnp.int32, (rows, width), 1)
    for head in range(heads):
        scaled = query_ref[:, head * width : (head + 1) * width] * jnp.bfloat16(HEAD ** (-0.5))
        for which in range(2):
            keep = (lane < HEAD) if which == 0 else (lane >= HEAD)
            spread[2 * head + which] = jnp.where(keep, scaled, jnp.zeros((), jnp.bfloat16))
    sums[...] = jnp.zeros_like(sums)
    peaks[...] = jnp.full_like(peaks, -1e30)
    start = start_ref[0]

    def step(block_index, masked):
        offset = pl.multiple_of(block_index * block_len, block_len)
        for head in range(heads):
            kv_head = head // group_size
            key_block = kv_ref[pl.ds(offset, block_len), kv_head * width : (kv_head + 1) * width]
            base = kv_heads * width + kv_head * VDIM
            value_block = kv_ref[pl.ds(offset, block_len), base : base + VDIM]
            extended = jnp.concatenate(
                [value_block, jnp.ones((block_len, VDIM), jnp.bfloat16)], axis=1
            )
            for which in range(2):
                slot = 2 * head + which
                scores = lax.dot_general(
                    spread[slot],
                    key_block,
                    (((1,), (1,)), ((), ())),
                    preferred_element_type=jnp.float32,
                )
                if masked:
                    query_pos = start + lax.broadcasted_iota(jnp.int32, scores.shape, 0)
                    key_pos = offset + lax.broadcasted_iota(jnp.int32, scores.shape, 1)
                    scores = jnp.where(key_pos <= query_pos, scores, -jnp.inf)
                old_peak = peaks[slot]
                new_peak = jnp.maximum(old_peak, jnp.max(scores, axis=-1, keepdims=True))
                peaks[slot] = new_peak
                factor = jnp.exp(old_peak - new_peak)
                weights = jnp.exp(scores - new_peak[:, :1]).astype(jnp.bfloat16)
                sums[slot] = sums[slot] * jnp.concatenate([factor, factor], axis=1) + jnp.dot(
                    weights, extended, preferred_element_type=jnp.float32
                )

    full = start // block_len

    def full_step(block_index, carry):
        step(block_index, False)
        return carry

    lax.fori_loop(0, full, full_step, 0)

    for extra in range(rows // block_len):
        step(full + extra, True)
    for head in range(heads):
        first, second = sums[2 * head], sums[2 * head + 1]
        combined = (
            first[:, :VDIM] / first[:, VDIM:]
            - lambda_ref[head] * second[:, :VDIM] / second[:, VDIM:]
        )
        inverse_rms = lax.rsqrt(jnp.mean(combined * combined, axis=-1, keepdims=True) + epsilon)
        out_ref[:, head * VDIM : (head + 1) * VDIM] = (
            combined * inverse_rms * gain_ref[...]
        ).astype(jnp.bfloat16)


def attention(queries, keys, values, head_lambda, out_gain):
    rows = queries.shape[0]
    heads = head_lambda.shape[0]
    block_len = math.gcd(rows, 512)
    gathered = lax.all_gather(jnp.concatenate([keys, values], axis=1), "ep", axis=0, tiled=True)
    start = (lax.axis_index("ep") * rows).astype(jnp.int32).reshape(1)
    return pl.pallas_call(
        functools.partial(attention_kernel, block_len),
        out_shape=jax.ShapeDtypeStruct((rows, heads * VDIM), jnp.bfloat16),
        in_specs=[
            pl.BlockSpec(memory_space=pltpu.SMEM),
            pl.BlockSpec(memory_space=pltpu.SMEM),
            pl.BlockSpec(memory_space=pltpu.VMEM),
            pl.BlockSpec(memory_space=pltpu.VMEM),
            pl.BlockSpec(memory_space=pltpu.VMEM),
        ],
        out_specs=pl.BlockSpec(memory_space=pltpu.VMEM),
        scratch_shapes=[
            pltpu.VMEM((2 * heads, rows, 2 * HEAD), jnp.bfloat16),
            pltpu.VMEM((2 * heads, rows, 2 * VDIM), jnp.float32),
            pltpu.VMEM((2 * heads, rows, VDIM), jnp.float32),
        ],
        cost_estimate=pl.CostEstimate(
            flops=16 * rows * gathered.shape[0] * heads * VDIM,
            bytes_accessed=8 * rows * gathered.shape[0],
            transcendentals=2 * rows * gathered.shape[0] * heads,
        ),
    )(start, head_lambda, queries, gathered, out_gain.reshape(1, VDIM))


def dense_experts(
    expert_input, routes, route_weight, moe_gain, gate_weight, up_weight, down_weight
):
    token_count, model_width = expert_input.shape
    ep_count = lax.axis_size("ep")
    chunks = CHUNKS
    inputs_f32 = expert_input.astype(jnp.float32)
    normed = (
        inputs_f32
        * lax.rsqrt(jnp.mean(inputs_f32 * inputs_f32, axis=-1, keepdims=True) + epsilon)
        * moe_gain
    ).astype(jnp.bfloat16)
    table = jnp.sum(
        jnp.where(
            routes[:, :, None] == jnp.arange(ep_count, dtype=jnp.int32)[None, None, :],
            route_weight[:, :, None],
            0.0,
        ),
        axis=1,
    )
    local_gate = gate_weight[0]
    local_up = up_weight[0]
    local_down = down_weight[0]
    both = ("ep", "tp")
    size = token_count // chunks
    arrived = [
        lax.all_gather(normed[at * size : (at + 1) * size], both, axis=0, tiled=True)
        for at in range(chunks)
    ]
    tables = lax.all_gather(table, both, axis=0, tiled=False)
    mine = lax.dynamic_index_in_dim(tables, lax.axis_index("ep"), 2, keepdims=False)
    mixed = []
    for at in range(chunks):
        activated = expert_act(arrived[at], local_gate, local_up)
        weight = mine[:, at * size : (at + 1) * size].reshape(-1, 1)
        product = jnp.dot(activated, local_down, preferred_element_type=jnp.float32)
        mixed.append(
            lax.psum_scatter(
                (product * weight).astype(jnp.bfloat16), both, scatter_dimension=0, tiled=True
            )
        )
    return jnp.concatenate(mixed, axis=0)


CHUNKS = 2


def shards(
    queries,
    keys,
    values,
    head_lambda,
    out_gain,
    expert_input,
    routes,
    route_weight,
    moe_gain,
    gate_weight,
    up_weight,
    down_weight,
):
    mixed_out = attention(queries, keys, values, head_lambda, out_gain)
    dense = lax.axis_size("ep") <= 2 * routes.shape[1]
    experts = dense_experts if dense else routed_experts
    expert_mix = experts(
        expert_input, routes, route_weight, moe_gain, gate_weight, up_weight, down_weight
    )
    return (mixed_out, expert_mix)


def solution(mesh):
    placed = (
        P("ep", "tp"),
        P("ep", "tp"),
        P("ep", "tp"),
        P("tp"),
        P(),
        P(("ep", "tp"), None),
        P(("ep", "tp"), None),
        P(("ep", "tp"), None),
        P(),
        P("ep", None, "tp"),
        P("ep", None, "tp"),
        P("ep", "tp", None),
    )
    return jax.shard_map(
        shards,
        mesh=mesh,
        in_specs=placed,
        out_specs=(P("ep", "tp"), P(("ep", "tp"), None)),
        check_vma=False,
    )
```

time: 420 us -> 528 us (1.26)
  the two profiles are of different devices: /device:TPU:28 before, /device:TPU:0 now
where the time goes in v1:
time: 528 us
  waiting for transfers between devices  416 us (79%)
  blocking collectives  43.7 us (8%)
  matrix products  40.2 us (8%)
  between operations  13.9 us (3%)
  other arithmetic  6.89 us (1%)
    reduce_scatter x2, waiting for transfers between devices, dense_experts(): lax.psum_scatter((product * weight).astype(jnp.bfloat16), both, scatter_d...  294 us
    all_gather x2, waiting for transfers between devices, dense_experts(): lax.all_gather(normed[at * size:(at + 1) * size], both, axis=0, tiled=True)  91.5 us
    all_gather x1, blocking collectives, dense_experts(): tables = lax.all_gather(table, both, axis=0, tiled=False)  43.7 us
    all_gather x1, waiting for transfers between devices, attention(): lax.all_gather(jnp.concatenate([keys, values], axis=1), 'ep', axis=0, til...  30.3 us
    dot_general x2, matrix products, expert_act(): up_pre = jnp.dot(rows_in, up_matrix, preferred_element_type=jnp.float32)  15.3 us
    dot_general x2, matrix products, dense_experts(): product = jnp.dot(activated, local_down, preferred_element_type=jnp.float32)  13.5 us
    dot_general x2, matrix products, expert_act(): gate_pre = jnp.dot(rows_in, gate_matrix, preferred_element_type=jnp.float32)  11.4 us
  transfers between devices with their start and end apart: 5, of which 5 were waited for; matrix products, arithmetic and copies ran while one was open for 8% of the time, Pallas kernels for 1%

profile of v1, /device:TPU:0, one launch (start us, length us, event | category | flops | bytes accessed | tf_op | source)
XLA Modules:
  0.0 527.6 jit_solution(567525862515672847)
XLA Ops:
  7.2 1.4 fusion.8
  8.6 1.2 fusion.10
  9.8 0.8 fusion.11
  10.8 0.7 all-gather.9.cloned.1.call-update
  11.5 1.7 pad_maximum_fusion.1
  13.3 0.7 select_reduce_fusion
  14.0 43.7 %all-gather = f32[4096,8]{0,1:T(8,128)S(1)} all-gather(f32[128,8]{0,1:T(8,128)S(1)} %select_reduce_fusion), channel_id=2, replica_groups=mesh['ep'=8,'tp'=4] {'ep','tp'}, dimensions={0}, use_global_device_ids=true | all-gather | bytes 135168 | tf_op jit(solution)/shard_map/all_gather | solution.py:203
  57.8 0.1 fusion.12
  57.8 0.1 mul.69
  57.9 33.5 %all-gather.7.cloned.1.call-done = bf16[2048,2048]{1,0:T(8,128)(2,1)} async-done(((bf16[64,2048]{1,0:T(8,128)(2,1)}), bf16[2048,2048]{1,0:T(8,128)(2,1)}) %all-gather.7.cloned.1.call-update) | async-done | bytes 8388624 | tf_op jit(solution)/shard_map/all_gather | solution.py:200
  91.4 7.7 %fusion.6 = f32[2048,512]{1,0:T(8,128)S(1)} fusion(bf16[2048,2048]{1,0:T(8,128)(2,1)} %all-gather.7.cloned.1.call-done, bf16[1,2048,512]{2,1,0:T(8,128)(2,1)} %param.22), kind=kOutput, calls=%fused_computation.10 | convolution fusion | flops 4294967296 | bytes 14680064 | tf_op jit(solution)/shard_map/dot_general | solution.py:22
  99.1 5.7 %multiply_convert_fusion.3 = bf16[2048,512]{1,0:T(8,128)(2,1)S(1)} fusion(f32[2048,512]{1,0:T(8,128)S(1)} %fusion.6, bf16[2048,2048]{1,0:T(8,128)(2,1)S(1)} %copy-done.2, bf16[1,2048,512]{2,1,0:T(8,128)(2,1)S(1)} %copy-done.3), kind=kOutput, calls=%fused_computation.3 | convolution fusion | flops 4305453056 | bytes 16777216 | tf_op jit(solution)/shard_map/dot_general | solution.py:21
  104.8 6.7 %multiply_convert_fusion.1 = bf16[2048,2048]{1,0:T(8,128)(2,1)} fusion(bf16[2048,512]{1,0:T(8,128)(2,1)S(1)} %multiply_convert_fusion.3, f32[2048]{0:T(1024)S(1)} %mul.69, bf16[1,512,2048]{2,1,0:T(8,128)(2,1)S(1)} %copy-done), kind=kOutput, calls=%fused_computation.1 | convolution fusion | flops 4303355904 | bytes 12591104 | tf_op jit(solution)/shard_map/dot_general | solution.py:209
  111.6 0.2 reduce-scatter.5.cloned.1.call-start
  111.8 0.1 mul.75
  111.9 58.1 %all-gather.9.cloned.1.call-done = bf16[2048,2048]{1,0:T(8,128)(2,1)} async-done(((bf16[64,2048]{1,0:T(8,128)(2,1)}), bf16[2048,2048]{1,0:T(8,128)(2,1)}) %all-gather.9.cloned.1.call-update) | async-done | bytes 8388624 | tf_op jit(solution)/shard_map/all_gather | solution.py:200
  169.9 7.7 %fusion.4 = f32[2048,512]{1,0:T(8,128)S(1)} fusion(bf16[2048,2048]{1,0:T(8,128)(2,1)} %all-gather.9.cloned.1.call-done, bf16[1,2048,512]{2,1,0:T(8,128)(2,1)} %param.22), kind=kOutput, calls=%fused_computation.8 | convolution fusion | flops 4294967296 | bytes 14680064 | tf_op jit(solution)/shard_map/dot_general | solution.py:22
  177.6 5.7 %multiply_convert_fusion.2 = bf16[2048,512]{1,0:T(8,128)(2,1)S(1)} fusion(f32[2048,512]{1,0:T(8,128)S(1)} %fusion.4, bf16[2048,2048]{1,0:T(8,128)(2,1)S(1)} %copy-done.1, bf16[1,2048,512]{2,1,0:T(8,128)(2,1)S(1)} %copy-done.4), kind=kOutput, calls=%fused_computation.2 | convolution fusion | flops 4305453056 | bytes 16777216 | tf_op jit(solution)/shard_map/dot_general | solution.py:21
  183.3 6.7 %multiply_convert_fusion = bf16[2048,2048]{1,0:T(8,128)(2,1)} fusion(bf16[2048,512]{1,0:T(8,128)(2,1)S(1)} %multiply_convert_fusion.2, f32[2048]{0:T(1024)S(1)} %mul.75, bf16[1,512,2048]{2,1,0:T(8,128)(2,1)S(1)} %copy-done), kind=kOutput, calls=%fused_computation | convolution fusion | flops 4303355904 | bytes 12591104 | tf_op jit(solution)/shard_map/dot_general | solution.py:209
  190.1 30.3 %all-gather.5.cloned.1.call-done.kv_ref = bf16[4096,256]{1,0:T(8,128)(2,1)} async-done(((bf16[512,256]{1,0:T(8,128)(2,1)}), bf16[4096,256]{1,0:T(8,128)(2,1)}) %all-gather.5.cloned.1.call-update) | async-done | bytes 2097168 | tf_op jit(solution)/shard_map/all_gather | solution.py:148
  220.4 5.0 shard_map.131
  225.4 145.7 %reduce-scatter.3.cloned.1.call-done = bf16[64,2048]{1,0:T(8,128)(2,1)} async-done(((bf16[2048,2048]{1,0:T(8,128)(2,1)}), bf16[64,2048]{1,0:T(8,128)(2,1)}) %reduce-scatter.3.cloned.1.call-update) | async-done | bytes 262160 | tf_op jit(solution)/shard_map/reduce_scatter | solution.py:211
  371.1 148.1 %reduce-scatter.5.cloned.1.call-done = bf16[64,2048]{1,0:T(8,128)(2,1)} async-done(((bf16[2048,2048]{1,0:T(8,128)(2,1)}), bf16[64,2048]{1,0:T(8,128)(2,1)}) %reduce-scatter.5.cloned.1.call-update) | async-done | bytes 262160 | tf_op jit(solution)/shard_map/reduce_scatter | solution.py:211
  519.2 1.9 pad_maximum_fusion
  (20 shorter events, 0.3 us)
Async XLA Ops:
  7.2 97.6 %copy-start = (bf16[1,512,2048]{2,1,0:T(8,128)(2,1)S(1)}, bf16[1,512,2048]{2,1,0:T(8,128)(2,1)}, u32[]{:S(2)}) copy-start(bf16[1,512,2048]{2,1,0:T(8,128)(2,1)} %param.23) | copy-start | bytes 6291460
  7.2 84.2 %all-gather.7.cloned.1.call-start = ((), (), s32[]{:S(2)}) async-start(), calls=%async_computation.3 | async-start | bytes 8650752 | tf_op jit(solution)/shard_map/all_gather | solution.py:200
  10.7 159.2 %all-gather.9.cloned.1.call-start = ((), (), s32[]{:S(2)}) async-start(), calls=%async_computation.5 | async-start | bytes 8650752 | tf_op jit(solution)/shard_map/all_gather | solution.py:200
  11.5 208.9 %all-gather.5.cloned.1.call-start = ((), (), s32[]{:S(2)}) async-start(), calls=%async_computation.2 | async-start | bytes 2359296 | tf_op jit(solution)/shard_map/all_gather | solution.py:148
  13.2 357.9 %reduce-scatter.3.cloned.1.call-start = ((), (), s32[]{:S(2)}) async-start(), calls=%async_computation.4 | async-start | bytes 8650752 | tf_op jit(solution)/shard_map/reduce_scatter | solution.py:211
  91.4 7.7 %copy-start.2 = (bf16[2048,2048]{1,0:T(8,128)(2,1)S(1)}, bf16[2048,2048]{1,0:T(8,128)(2,1)}, u32[]{:S(2)}) copy-start(bf16[2048,2048]{1,0:T(8,128)(2,1)} %all-gather.7.cloned.1.call-done) | copy-start | bytes 25165828
  91.4 7.7 %copy-start.3 = (bf16[1,2048,512]{2,1,0:T(8,128)(2,1)S(1)}, bf16[1,2048,512]{2,1,0:T(8,128)(2,1)}, u32[]{:S(2)}) copy-start(bf16[1,2048,512]{2,1,0:T(8,128)(2,1)} %param.21) | copy-start | bytes 6291460
  111.6 407.6 %reduce-scatter.5.cloned.1.call-start = ((), (), s32[]{:S(2)}) async-start(), calls=%async_computation.6 | async-start | bytes 8650752 | tf_op jit(solution)/shard_map/reduce_scatter | solution.py:211
  169.9 7.7 %copy-start.1 = (bf16[2048,2048]{1,0:T(8,128)(2,1)S(1)}, bf16[2048,2048]{1,0:T(8,128)(2,1)}, u32[]{:S(2)}) copy-start(bf16[2048,2048]{1,0:T(8,128)(2,1)} %all-gather.9.cloned.1.call-done) | copy-start | bytes 25165828
  169.9 7.7 %copy-start.4 = (bf16[1,2048,512]{2,1,0:T(8,128)(2,1)S(1)}, bf16[1,2048,512]{2,1,0:T(8,128)(2,1)}, u32[]{:S(2)}) copy-start(bf16[1,2048,512]{2,1,0:T(8,128)(2,1)} %param.21) | copy-start | bytes 6291460
Sparse Core Ops, SparseCore 0:
  11.4 79.8 all-gather.6
  94.2 75.6 all-gather.8
  172.6 47.6 all-gather.4
  222.5 148.5 reduce-scatter.2
  373.2 145.9 reduce-scatter.4

commit v2 on v1

--- a/solution.py
+++ b/solution.py
@@ -26,7 +26,7 @@
 
 
 def routed_experts(
-    expert_input, routes, route_weight, moe_gain, gate_weight, up_weight, down_weight
+    kv_gathered, expert_input, routes, route_weight, moe_gain, gate_weight, up_weight, down_weight
 ):
     token_count = expert_input.shape[0]
     top_count = routes.shape[1]
@@ -56,18 +56,44 @@
     local_gate = gate_weight[0]
     local_up = up_weight[0]
     local_down = down_weight[0]
-    arrived = lax.all_to_all(outgoing, "ep", split_axis=0, concat_axis=0, tiled=True)
-    activated = expert_act(lax.all_gather(arrived, "tp", axis=0, tiled=True), local_gate, local_up)
-    summed = lax.psum_scatter(
-        jnp.dot(activated, local_down, preferred_element_type=jnp.float32).astype(jnp.bfloat16),
-        "tp",
-        scatter_dimension=0,
-        tiled=True,
-    )
-    returned = lax.all_to_all(summed, "ep", split_axis=0, concat_axis=0, tiled=True)
-    picked = returned[target].reshape(token_count, top_count, model_width).astype(jnp.float32)
-    expert_mix = jnp.sum(route_weight[:, :, None] * picked, axis=1).astype(jnp.bfloat16)
-    return expert_mix
+    parts = 2 if capacity % 16 == 0 else 1
+    share = capacity // parts
+    by_expert = outgoing.reshape(ep_count, capacity, model_width)
+    gathered = []
+    for part in range(parts):
+        sending = by_expert[:, part * share : (part + 1) * share].reshape(-1, model_width)
+        arrived = lax.all_to_all(sending, "ep", split_axis=0, concat_axis=0, tiled=True)
+        if part == 0:
+            arrived, kv_gathered = lax.optimization_barrier((arrived, kv_gathered))
+        gathered.append(lax.all_gather(arrived, "tp", axis=0, tiled=True))
+    summed = []
+    for rows_in in gathered:
+        activated = expert_act(rows_in, local_gate, local_up)
+        summed.append(
+            lax.psum_scatter(
+                jnp.dot(activated, local_down, preferred_element_type=jnp.float32).astype(
+                    jnp.bfloat16
+                ),
+                "tp",
+                scatter_dimension=0,
+                tiled=True,
+            )
+        )
+    returned = jnp.concatenate(
+        [
+            lax.all_to_all(piece, "ep", split_axis=0, concat_axis=0, tiled=True)
+            for piece in summed
+        ],
+        axis=0,
+    )
+    part_of = slot_rank // share
+    place = part_of * (ep_count * share) + flat_routes * share + slot_rank % share
+    by_choice = place.reshape(token_count, top_count).T.reshape(-1)
+    picked = returned[by_choice].reshape(top_count, token_count, model_width)
+    expert_mix = jnp.sum(
+        route_weight.T[:, :, None] * picked.astype(jnp.float32), axis=0
+    ).astype(jnp.bfloat16)
+    return kv_gathered, expert_mix
 
 
 def attention_kernel(
@@ -141,11 +167,10 @@
         ).astype(jnp.bfloat16)
 
 
-def attention(queries, keys, values, head_lambda, out_gain):
+def attention(queries, gathered, head_lambda, out_gain):
     rows = queries.shape[0]
     heads = head_lambda.shape[0]
     block_len = math.gcd(rows, 512)
-    gathered = lax.all_gather(jnp.concatenate([keys, values], axis=1), "ep", axis=0, tiled=True)
     start = (lax.axis_index("ep") * rows).astype(jnp.int32).reshape(1)
     return pl.pallas_call(
         functools.partial(attention_kernel, block_len),
@@ -171,53 +196,6 @@
     )(start, head_lambda, queries, gathered, out_gain.reshape(1, VDIM))
 
 
-def dense_experts(
-    expert_input, routes, route_weight, moe_gain, gate_weight, up_weight, down_weight
-):
-    token_count, model_width = expert_input.shape
-    ep_count = lax.axis_size("ep")
-    chunks = CHUNKS
-    inputs_f32 = expert_input.astype(jnp.float32)
-    normed = (
-        inputs_f32
-        * lax.rsqrt(jnp.mean(inputs_f32 * inputs_f32, axis=-1, keepdims=True) + epsilon)
-        * moe_gain
-    ).astype(jnp.bfloat16)
-    table = jnp.sum(
-        jnp.where(
-            routes[:, :, None] == jnp.arange(ep_count, dtype=jnp.int32)[None, None, :],
-            route_weight[:, :, None],
-            0.0,
-        ),
-        axis=1,
-    )
-    local_gate = gate_weight[0]
-    local_up = up_weight[0]
-    local_down = down_weight[0]
-    both = ("ep", "tp")
-    size = token_count // chunks
-    arrived = [
-        lax.all_gather(normed[at * size : (at + 1) * size], both, axis=0, tiled=True)
-        for at in range(chunks)
-    ]
-    tables = lax.all_gather(table, both, axis=0, tiled=False)
-    mine = lax.dynamic_index_in_dim(tables, lax.axis_index("ep"), 2, keepdims=False)
-    mixed = []
-    for at in range(chunks):
-        activated = expert_act(arrived[at], local_gate, local_up)
-        weight = mine[:, at * size : (at + 1) * size].reshape(-1, 1)
-        product = jnp.dot(activated, local_down, preferred_element_type=jnp.float32)
-        mixed.append(
-            lax.psum_scatter(
-                (product * weight).astype(jnp.bfloat16), both, scatter_dimension=0, tiled=True
-            )
-        )
-    return jnp.concatenate(mixed, axis=0)
-
-
-CHUNKS = 2
-
-
 def shards(
     queries,
     keys,
@@ -232,12 +210,13 @@
     up_weight,
     down_weight,
 ):
-    mixed_out = attention(queries, keys, values, head_lambda, out_gain)
-    dense = lax.axis_size("ep") <= 2 * routes.shape[1]
-    experts = dense_experts if dense else routed_experts
-    expert_mix = experts(
-        expert_input, routes, route_weight, moe_gain, gate_weight, up_weight, down_weight
-    )
+    kv_gathered = lax.all_gather(
+        jnp.concatenate([keys, values], axis=1), "ep", axis=0, tiled=True
+    )
+    kv_gathered, expert_mix = routed_experts(
+        kv_gathered, expert_input, routes, route_weight, moe_gain, gate_weight, up_weight, down_weight
+    )
+    mixed_out = attention(queries, kv_gathered, head_lambda, out_gain)
     return (mixed_out, expert_mix)
 
 

time: 528 us -> 329 us (0.62)
  waiting for transfers between devices: 416 us -> 138 us
  blocking collectives: 43.7 us -> 90 us
  local copies, waits for them, and re-layouts: 1.09 us -> 18.7 us
  starting transfers between devices: 0.38 us -> 11.4 us
  other arithmetic: 6.89 us -> 14.4 us
    reduce_scatter x2, waiting for transfers between devices: 294 us -> 83.9 us  [routed_experts(): lax.psum_scatter(jnp.dot(activated, local_down, preferred_element_type=jn...]
    all_gather x3, waiting for transfers between devices: 122 us -> 28 us  [the longest x2 28 us: routed_experts(): gathered.append(lax.all_gather(arrived, 'tp', axis=0, tiled=True))]
    all_to_all x0 -> x2, blocking collectives: none -> 90 us  [routed_experts(): lax.all_to_all(sending, 'ep', split_axis=0, concat_axis=0, tiled=True)]
    all_gather x1 -> x0, blocking collectives: 43.7 us -> none  [dense_experts(): tables = lax.all_gather(table, both, axis=0, tiled=False)]
    all_to_all x0 -> x2, waiting for transfers between devices: none -> 26.1 us  [routed_experts(): lax.all_to_all(piece, 'ep', split_axis=0, concat_axis=0, tiled=True)]
    gather x0 -> x2, local copies, waits for them, and re-layouts: none -> 11.4 us  [the longest x1 7.3 us: routed_experts(): picked = returned[by_choice].reshape(top_count, token_count, model_width)]
    all_to_all x0 -> x2, starting transfers between devices: none -> 11 us  [routed_experts(): lax.all_to_all(piece, 'ep', split_axis=0, concat_axis=0, tiled=True)]
    dot_general x4 -> x2, matrix products: 28.8 us -> 21.8 us  [routed_experts(): jnp.dot(activated, local_down, preferred_element_type=jnp.float32)]
  transfers between devices with their start and end apart: 5 -> 7, of which waited for: 5 -> 5; matrix products, arithmetic and copies ran while one was open for 8% -> 17% of each run, Pallas kernels for 1% -> 2%
where the time goes in v2:
time: 329 us
  waiting for transfers between devices  138 us (42%)
  blocking collectives  90 us (27%)
  matrix products  36.8 us (11%)
  local copies, waits for them, and re-layouts  18.7 us (6%)
  other arithmetic  14.4 us (4%)
  between operations  13.9 us (4%)
  starting transfers between devices  11.4 us (3%)
  Pallas kernels  5.22 us (2%)
    all_to_all x2, blocking collectives, routed_experts(): lax.all_to_all(sending, 'ep', split_axis=0, concat_axis=0, tiled=True)  90 us
    reduce_scatter x2, waiting for transfers between devices, routed_experts(): lax.psum_scatter(jnp.dot(activated, local_down, preferred_element_type=jn...  83.9 us
    all_gather x2, waiting for transfers between devices, routed_experts(): gathered.append(lax.all_gather(arrived, 'tp', axis=0, tiled=True))  28 us
    all_to_all x2, waiting for transfers between devices, routed_experts(): lax.all_to_all(piece, 'ep', split_axis=0, concat_axis=0, tiled=True)  26.1 us
    dot_general x2, matrix products, routed_experts(): jnp.dot(activated, local_down, preferred_element_type=jnp.float32)  21.8 us
    dot_general x2, matrix products, expert_act(): gate_pre = jnp.dot(rows_in, gate_matrix, preferred_element_type=jnp.float32)  15 us
    all_to_all x2, starting transfers between devices, routed_experts(): lax.all_to_all(piece, 'ep', split_axis=0, concat_axis=0, tiled=True)  11 us
    gather x1, local copies, waits for them, and re-layouts, routed_experts(): picked = returned[by_choice].reshape(top_count, token_count, model_width)  7.3 us
  transfers between devices with their start and end apart: 7, of which 5 were waited for; matrix products, arithmetic and copies ran while one was open for 17% of the time, Pallas kernels for 2%

profile of v2, /device:TPU:0, one launch (start us, length us, event | category | flops | bytes accessed | tf_op | source)
XLA Modules:
  0.0 328.5 jit_solution(8216438752315138700)
XLA Ops:
  7.2 1.8 pad_maximum_fusion.1
  11.7 1.2 fusion.15
  14.5 2.4 scatter_custom_fusion.1
  16.9 2.4 scatter_custom_fusion
  19.5 1.3 fusion.17
  20.8 4.1 %gather_fusion = bf16[640,2048]{1,0:T(8,128)(2,1)} fusion(bf16[128,2048]{1,0:T(8,128)(2,1)S(1)} %fusion.17, s32[1024]{0:T(1024)S(1)} %pad_clamp_fusion.1), kind=kCustom, calls=%fused_computation | custom fusion | bytes 5245440 | tf_op jit(solution)/shard_map/gather | solution.py:55
  24.9 2.0 broadcast_select_fusion
  27.2 55.5 %all_to_all.42 = bf16[8,40,2048]{2,1,0:T(8,128)(2,1)} all-to-all(bf16[8,40,2048]{2,1,0:T(8,128)(2,1)S(1)} %get-tuple-element.6), channel_id=1, replica_groups=mesh['ep'=8,'tp'=4] {'ep'}, dimensions={0} | all-to-all | bytes 2621440 | tf_op jit(solution)/shard_map/all_to_all | solution.py:65
  82.7 34.6 %all_to_all.43 = bf16[8,40,2048]{2,1,0:T(8,128)(2,1)} all-to-all(bf16[8,40,2048]{2,1,0:T(8,128)(2,1)S(1)} %get-tuple-element.7), channel_id=1, replica_groups=mesh['ep'=8,'tp'=4] {'ep'}, dimensions={0} | all-to-all | bytes 2621440 | tf_op jit(solution)/shard_map/all_to_all | solution.py:65
  117.4 4.9 %all-gather.8.cloned.1.call-done = bf16[1280,2048]{1,0:T(8,128)(2,1)} async-done(((bf16[320,2048]{1,0:T(8,128)(2,1)}), bf16[1280,2048]{1,0:T(8,128)(2,1)}) %all-gather.8.cloned.1.call-update) | async-done | bytes 5242896 | tf_op jit(solution)/shard_map/all_gather | solution.py:68
  122.2 7.5 %convolution_minimum_fusion = f32[1280,512]{1,0:T(8,128)} fusion(bf16[1280,2048]{1,0:T(8,128)(2,1)} %all-gather.8.cloned.1.call-done, bf16[1,2048,512]{2,1,0:T(8,128)(2,1)} %param.21), kind=kOutput, calls=%fused_computation.10 | convolution fusion | flops 2685009920 | bytes 9961472 | tf_op jit(solution)/shard_map/dot_general | solution.py:21
  129.7 11.1 %convolution_convert_fusion = bf16[1280,2048]{1,0:T(8,128)(2,1)} fusion(bf16[1,512,2048]{2,1,0:T(8,128)(2,1)S(1)} %copy-done, f32[1280,512]{1,0:T(8,128)} %convolution_minimum_fusion, bf16[1280,2048]{1,0:T(8,128)(2,1)} %all-gather.8.cloned.1.call-done, bf16[1,2048,512]{2,1,0:T(8,128)(2,1)} %param.22), kind=kOutput, calls=%fused_computation.4 | convolution fusion | flops 5377228800 | bytes 17301504 | tf_op jit(solution)/shard_map/dot_general | solution.py:74
  141.1 23.1 %all-gather.6.cloned.1.call-done = bf16[1280,2048]{1,0:T(8,128)(2,1)} async-done(((bf16[320,2048]{1,0:T(8,128)(2,1)}), bf16[1280,2048]{1,0:T(8,128)(2,1)}) %all-gather.6.cloned.1.call-update) | async-done | bytes 5242896 | tf_op jit(solution)/shard_map/all_gather | solution.py:68
  164.2 7.5 %convolution_minimum_fusion.1 = f32[1280,512]{1,0:T(8,128)} fusion(bf16[1280,2048]{1,0:T(8,128)(2,1)} %all-gather.6.cloned.1.call-done, bf16[1,2048,512]{2,1,0:T(8,128)(2,1)} %param.21), kind=kOutput, calls=%fused_computation.11 | convolution fusion | flops 2685009920 | bytes 9961472 | tf_op jit(solution)/shard_map/dot_general | solution.py:21
  171.8 10.6 %convolution_convert_fusion.1 = bf16[1280,2048]{1,0:T(8,128)(2,1)} fusion(bf16[1,512,2048]{2,1,0:T(8,128)(2,1)S(1)} %copy-done, f32[1280,512]{1,0:T(8,128)} %convolution_minimum_fusion.1, bf16[1280,2048]{1,0:T(8,128)(2,1)} %all-gather.6.cloned.1.call-done, bf16[1,2048,512]{2,1,0:T(8,128)(2,1)} %param.22), kind=kOutput, calls=%fused_computation.5 | convolution fusion | flops 5377228800 | bytes 17301504 | tf_op jit(solution)/shard_map/dot_general | solution.py:74
  182.4 35.6 %reduce-scatter.5.cloned.1.call-done = bf16[320,2048]{1,0:T(8,128)(2,1)} async-done(((bf16[1280,2048]{1,0:T(8,128)(2,1)}), bf16[320,2048]{1,0:T(8,128)(2,1)}) %reduce-scatter.5.cloned.1.call-update) | async-done | bytes 1310736 | tf_op jit(solution)/shard_map/reduce_scatter | solution.py:73
  218.0 5.5 %all-to-all-start.3 = ((bf16[8,40,2048]{2,1,0:T(8,128)(2,1)}), bf16[8,40,2048]{2,1,0:T(8,128)(2,1)S(1)}, u32[]{:S(2)}, u32[]{:S(2)}) async-start(bf16[8,40,2048]{2,1,0:T(8,128)(2,1)} %bitcast.53), calls=%async_computation.5 | async-start | bytes 2621440 | tf_op jit(solution)/shard_map/all_to_all | solution.py:84
  223.5 48.3 %reduce-scatter.3.cloned.1.call-done = bf16[320,2048]{1,0:T(8,128)(2,1)} async-done(((bf16[1280,2048]{1,0:T(8,128)(2,1)}), bf16[320,2048]{1,0:T(8,128)(2,1)}) %reduce-scatter.3.cloned.1.call-update) | async-done | bytes 1310736 | tf_op jit(solution)/shard_map/reduce_scatter | solution.py:73
  271.8 5.5 %all-to-all-start.1 = ((bf16[8,40,2048]{2,1,0:T(8,128)(2,1)}), bf16[8,40,2048]{2,1,0:T(8,128)(2,1)}, u32[]{:S(2)}, u32[]{:S(2)}) async-start(bf16[8,40,2048]{2,1,0:T(8,128)(2,1)} %bitcast.52), calls=%async_computation.2 | async-start | bytes 2621440 | tf_op jit(solution)/shard_map/all_to_all | solution.py:84
  277.3 5.2 %shard_map.131 = bf16[512,256]{1,0:T(8,128)(2,1)} custom-call(s32[1]{0:T(128)} %bitcast.start_ref, f32[2]{0:T(128)} %lambda_ref.1, bf16[512,256]{1,0:T(8,128)(2,1)} %query_ref.1, bf16[4096,256]{1,0:T(8,128)(2,1)} %all-gather.4.cloned.1.call-done.kv_ref, f32[1,128]{1,0:T(1,128)} %bitcast.60), custom_call_target="tpu_custom_call" | custom-call | flops 8589934592 | bytes 16777216 | tf_op jit(solution)/shard_map/pallas_call | solution.py:175
  282.6 26.1 %all-to-all-done.1 = bf16[8,40,2048]{2,1,0:T(8,128)(2,1)} async-done(((bf16[8,40,2048]{2,1,0:T(8,128)(2,1)}), bf16[8,40,2048]{2,1,0:T(8,128)(2,1)}, u32[]{:S(2)}, u32[]{:S(2)}) %all-to-all-start.1) | async-done | bytes 1310752 | tf_op jit(solution)/shard_map/all_to_all | solution.py:84
  308.6 3.1 pad_maximum_fusion
  311.7 7.3 %gather_fusion.1 = bf16[512,2048]{1,0:T(8,128)(2,1)} fusion(bf16[640,2048]{1,0:T(8,128)(2,1)} %pad_maximum_fusion, s32[1024]{0:T(1024)S(1)} %pad_clamp_fusion), kind=kCustom, calls=%fused_computation.1 | custom fusion | bytes 4196352 | tf_op jit(solution)/shard_map/gather | solution.py:92
  319.0 3.0 fusion
  (46 shorter events, 5.0 us)
Async XLA Ops:
  7.2 122.6 %copy-start = (bf16[1,512,2048]{2,1,0:T(8,128)(2,1)S(1)}, bf16[1,512,2048]{2,1,0:T(8,128)(2,1)}, u32[]{:S(2)}) copy-start(bf16[1,512,2048]{2,1,0:T(8,128)(2,1)} %param.23) | copy-start | bytes 6291460
  7.2 110.1 %all-gather.4.cloned.1.call-start = ((), (), s32[]{:S(2)}) async-start(), calls=%async_computation.6 | async-start | bytes 2359296 | tf_op jit(solution)/shard_map/all_gather | solution.py:213
  9.1 113.1 %all-gather.8.cloned.1.call-start = ((), (), s32[]{:S(2)}) async-start(), calls=%async_computation.9 | async-start | bytes 6553600 | tf_op jit(solution)/shard_map/all_gather | solution.py:68
  82.7 81.6 %all-gather.6.cloned.1.call-start = ((), (), s32[]{:S(2)}) async-start(), calls=%async_computation.7 | async-start | bytes 6553600 | tf_op jit(solution)/shard_map/all_gather | solution.py:68
  117.3 100.7 %reduce-scatter.5.cloned.1.call-start = ((), (), s32[]{:S(2)}) async-start(), calls=%async_computation.10 | async-start | bytes 6553600 | tf_op jit(solution)/shard_map/reduce_scatter | solution.py:73
  140.9 130.9 %reduce-scatter.3.cloned.1.call-start = ((), (), s32[]{:S(2)}) async-start(), calls=%async_computation.8 | async-start | bytes 6553600 | tf_op jit(solution)/shard_map/reduce_scatter | solution.py:73
  218.0 53.8 %all-to-all-start.3 = ((bf16[8,40,2048]{2,1,0:T(8,128)(2,1)}), bf16[8,40,2048]{2,1,0:T(8,128)(2,1)S(1)}, u32[]{:S(2)}, u32[]{:S(2)}) async-start(bf16[8,40,2048]{2,1,0:T(8,128)(2,1)} %bitcast.53), calls=%async_computation.5 | async-start | bytes 2621440 | tf_op jit(solution)/shard_map/all_to_all | solution.py:84
  271.8 36.8 %all-to-all-start.1 = ((bf16[8,40,2048]{2,1,0:T(8,128)(2,1)}), bf16[8,40,2048]{2,1,0:T(8,128)(2,1)}, u32[]{:S(2)}, u32[]{:S(2)}) async-start(bf16[8,40,2048]{2,1,0:T(8,128)(2,1)} %bitcast.52), calls=%async_computation.2 | async-start | bytes 2621440 | tf_op jit(solution)/shard_map/all_to_all | solution.py:84
  311.7 7.3 %copy-start.1 = (f32[128,4]{0,1:T(4,128)S(1)}, f32[128,4]{0,1:T(4,128)}, u32[]{:S(2)}) copy-start(f32[128,4]{0,1:T(4,128)} %param.19) | copy-start | bytes 6148
Sparse Core Ops, SparseCore 0:
  10.7 69.5 all-gather.3
  82.8 39.4 all-gather.7
  123.8 40.3 all-gather.5
  166.6 51.3 reduce-scatter.4
  220.4 51.3 reduce-scatter.2
